TPU v7x, 512 devices: a whole 4x4x16 slice. The times are simulated.
512 devices in a mesh: ep: 32 (over z, core), tp: 16 (over y, x).
Axes of the slice: x: 4, y: 4, z: 16, core: 2. Of those that a mesh axis runs over, the one named last changes fastest.
Arguments:
- queries: bfloat16 [8192, 2048], P('ep', 'tp'), may hold values from -6 to 6
- key_rows: bfloat16 [8192, 1024], P('ep', 'tp'), may hold values from -6 to 6
- values: bfloat16 [8192, 1024], P('ep', 'tp'), may hold values from -140 to 140
- query_gain: float32 [64], replicated, may hold values from 0.55 to 7.5
- key_gain: float32 [64], replicated, may hold values from 0.55 to 7.5
- mix_gain: float32 [2048], replicated, may hold values from 0.1 to 1.9
- out_weight: bfloat16 [2048, 4096], P(None, 'tp'), may hold values from -0.125 to 0.125
- expert_input: bfloat16 [8192, 4096], P('ep', 'tp'), may hold values from -140 to 140
- expert_gain: float32 [4096], replicated, may hold values from 0.1 to 1.9
- route_ids: int32 [8192, 2], P('ep'), may hold values from 0 to 31, as said below
- route_weights: float32 [8192, 2], P('ep'), may hold values from 0.3 to 1.7
- expert_gate: bfloat16 [32, 4096, 2048], P('ep', None, 'tp'), may hold values from -0.09375 to 0.09375
- expert_up: bfloat16 [32, 4096, 2048], P('ep', None, 'tp'), may hold values from -0.09375 to 0.09375
- expert_down: bfloat16 [32, 2048, 4096], P('ep', None, 'tp'), may hold values from -0.125 to 0.125
Outputs:
- attended: bfloat16 [8192, 4096], P('ep', 'tp')
- expert_mix: bfloat16 [8192, 4096], P('ep', 'tp')
Inputs may be any that keep to these rules, and one draw needn't show every extreme that they name: `route_ids`: the 2 experts of a row differ. In every aligned block of 256 rows no expert is named more than 22 times, and one expert, the same for all blocks, is named exactly 22 times in every block.
All inputs are finite; a program needn't handle non-finite values.
Results may differ from a plain program's by a relative error of at most 0.01.
The roundings to bfloat16 on the way count: a program that leaves them out, or rounds other values in their place, can miss the bound.
Values may be sent and summed in bfloat16 or wider, within the bound.
A program may use at most 64 MiB of HBM per device.

v0:
```python
import math

import jax
import jax.numpy as jnp
from jax import lax
from jax.sharding import Mesh
from jax.sharding import PartitionSpec as P

Q_HEADS = 32
KV_HEADS = 16
HEAD = 64
GRID_W = 64
EP = ("ep_0", "ep_1")


EPS = 1e-06
THETA = 10000.0


def in_one_piece(arrays, axis, dim, along):
    widths = [a.shape[along] for a in arrays]
    both = jnp.concatenate(arrays, axis=along)
    filled = lax.all_gather(both, axis, axis=dim, tiled=True)
    return tuple(jnp.split(filled, [sum(widths[:k]) for k in range(1, len(widths))], axis=along))


def split_up(array, dim, length):
    before, after = (array.shape[:dim], array.shape[dim + 1 :])
    return jnp.moveaxis(array.reshape(*before, length, -1, *after), dim, 0)


def joined_along(blocks, dim):
    lengths = list(blocks.shape[1:])
    lengths[dim] *= blocks.shape[0]
    return jnp.moveaxis(blocks, 0, dim).reshape(lengths)


def exchange_in_order(blocks, axes, order):
    inside = blocks.shape[1:]
    filled = blocks.reshape(*(lax.axis_size(a) for a in axes), *inside)
    for k in order:
        filled = lax.all_to_all(filled, axes[k], k, k, tiled=True)
    return filled.reshape(-1, *inside)


def exchange_by_chip(array, groups, order, split_dim, concat_dim):
    length = lax.axis_size(groups[0]) * lax.axis_size(groups[1])
    blocks = split_up(array, split_dim, length)
    return joined_along(exchange_in_order(blocks, groups, order), concat_dim)


def turn_tables(offset, length):
    half_width = HEAD // 2
    inverse = THETA ** (-jnp.arange(0, half_width, 2, dtype=jnp.float32) / half_width)
    positions = offset + jnp.arange(length, dtype=jnp.int32)
    grid_rows = (positions // GRID_W).astype(jnp.float32)
    grid_cols = (positions % GRID_W).astype(jnp.float32)
    angles = jnp.concatenate([grid_rows[:, None] * inverse, grid_cols[:, None] * inverse], axis=-1)
    return (jnp.cos(angles), jnp.sin(angles))


def norm_turn(source, scale_gain, cosine_table, sine_table):
    length = source.shape[0]
    head_rows = source.astype(jnp.float32).reshape(length, -1, HEAD)
    head_rows = (
        head_rows
        * lax.rsqrt(jnp.mean(head_rows * head_rows, axis=-1, keepdims=True) + EPS)
        * scale_gain
    )
    pair_view = head_rows.reshape(length, head_rows.shape[1], HEAD // 2, 2)
    even_part = pair_view[..., 0]
    odd_part = pair_view[..., 1]
    cosine_part = cosine_table[:, None, :]
    sine_part = sine_table[:, None, :]
    turned = jnp.stack(
        [
            even_part * cosine_part - odd_part * sine_part,
            even_part * sine_part + odd_part * cosine_part,
        ],
        axis=-1,
    )
    return turned.reshape(length, -1).astype(jnp.bfloat16)


def shards(
    queries,
    key_rows,
    values,
    query_gain,
    key_gain,
    mix_gain,
    out_weight,
    expert_input,
    expert_gain,
    route_ids,
    route_weights,
    expert_gate,
    expert_up,
    expert_down,
):
    length = queries.shape[0]
    experts_count = lax.axis_size(EP)
    offset = lax.axis_index(EP) * length
    cosine_table, sine_table = turn_tables(offset, length)
    query_turned = norm_turn(queries, query_gain, cosine_table, sine_table)
    key_turned = norm_turn(key_rows, key_gain, cosine_table, sine_table)
    kv_local = key_rows.shape[1] // HEAD
    group_size = Q_HEADS // KV_HEADS
    query_heads = query_turned.reshape(length, kv_local, group_size, HEAD)
    start_state = (
        jnp.full((kv_local, group_size, length), -jnp.inf, jnp.float32),
        jnp.zeros((kv_local, group_size, length), jnp.float32),
        jnp.zeros((length, kv_local, group_size, HEAD), jnp.float32),
    )
    key_piece, value_piece = in_one_piece((key_turned, values), EP, 0, 1)
    piece_rows = key_piece.shape[0]
    step_rows = 1024
    key_blocks = key_piece.reshape(piece_rows // step_rows, step_rows, kv_local, HEAD)
    value_blocks = value_piece.reshape(piece_rows // step_rows, step_rows, kv_local, HEAD)

    def absorb(current, block_pair):
        running_max, running_sum, running_acc = current
        key_block, value_block = block_pair
        scores = jnp.einsum(
            "rhgd,nhd->hgrn", query_heads, key_block, preferred_element_type=jnp.float32
        ) / math.sqrt(HEAD)
        new_max = jnp.maximum(running_max, jnp.max(scores, axis=-1))
        factor = jnp.exp(running_max - new_max)
        raw_weights = jnp.exp(scores - new_max[..., None])
        new_sum = running_sum * factor + jnp.sum(raw_weights, axis=-1)
        rounded = raw_weights.astype(jnp.bfloat16)
        increment = jnp.einsum(
            "hgrn,nhd->rhgd", rounded, value_block, preferred_element_type=jnp.float32
        )
        new_acc = running_acc * jnp.transpose(factor, (2, 0, 1))[..., None] + increment
        return ((new_max, new_sum, new_acc), None)

    result, unused = lax.scan(absorb, start_state, (key_blocks, value_blocks))
    heads_out = (
        (result[2] / jnp.transpose(result[1], (2, 0, 1))[..., None])
        .reshape(length, -1)
        .astype(jnp.bfloat16)
    )
    top_count = route_ids.shape[1]
    copies = route_ids.shape[0] * top_count
    capacity = (4 * copies + 3 * experts_count - 1) // (3 * experts_count)
    slot_total = experts_count * capacity
    flat_ids = route_ids.reshape(copies)
    hit_marks = (flat_ids[:, None] == jnp.arange(experts_count, dtype=jnp.int32)[None, :]).astype(
        jnp.int32
    )
    earlier = jnp.cumsum(hit_marks, axis=0) - hit_marks
    places = jnp.sum(earlier * hit_marks, axis=1)
    slot_index = flat_ids * capacity + places
    slot_rows = (
        jnp.full((slot_total,), route_ids.shape[0], jnp.int32)
        .at[slot_index]
        .set(jnp.arange(copies, dtype=jnp.int32) // top_count)
    )
    width_local = expert_input.shape[1]
    padded = jnp.concatenate([expert_input, jnp.zeros((1, width_local), jnp.bfloat16)], axis=0)
    outgoing = padded[slot_rows].reshape(experts_count, capacity, width_local)
    arrived = exchange_by_chip(outgoing, ("ep_0", "ep_1"), (1, 0), 0, 0).reshape(
        slot_total, width_local
    )
    piece_float = lax.all_gather(arrived, "tp", axis=1, tiled=True).astype(jnp.float32)
    gain_piece = expert_gain
    scaled_piece = (piece_float * gain_piece).astype(jnp.bfloat16)
    gate_rows = expert_gate[0]
    up_rows = expert_up[0]
    gate_sum = jnp.dot(scaled_piece, gate_rows, preferred_element_type=jnp.float32)
    up_sum = jnp.dot(scaled_piece, up_rows, preferred_element_type=jnp.float32)
    square_sum = jnp.sum(piece_float * piece_float, axis=1)
    row_stat = lax.rsqrt(square_sum / expert_gain.shape[0] + EPS)
    gate_value = gate_sum * row_stat[:, None]
    up_value = up_sum * row_stat[:, None]
    hidden = (jax.nn.silu(gate_value) * up_value).astype(jnp.bfloat16)
    width_out = out_weight.shape[1]
    head_piece, hidden_piece = in_one_piece((heads_out, hidden), "tp", 1, 0)
    head_float = head_piece.astype(jnp.float32)
    gain_piece = mix_gain
    mix_in = (head_float * gain_piece).astype(jnp.bfloat16)
    down_rows = expert_down[0]
    mix_sum = jnp.dot(mix_in, out_weight, preferred_element_type=jnp.float32)
    mix_squares = jnp.sum(head_float * head_float, axis=1)
    expert_sum = jnp.dot(hidden_piece, down_rows, preferred_element_type=jnp.float32)
    attended = (mix_sum * lax.rsqrt(mix_squares / mix_gain.shape[0] + EPS)[:, None]).astype(
        jnp.bfloat16
    )
    expert_back = expert_sum.astype(jnp.bfloat16).reshape(experts_count, capacity, width_out)
    returned = lax.all_to_all(expert_back, EP, split_axis=0, concat_axis=0, tiled=True).reshape(
        slot_total, width_out
    )
    picked = returned[slot_index].astype(jnp.float32) * route_weights.reshape(copies)[:, None]
    expert_mix = jnp.sum(picked.reshape(route_ids.shape[0], top_count, width_out), axis=1).astype(
        jnp.bfloat16
    )
    return (attended, expert_mix)


def solution(mesh):
    torus = Mesh(mesh.devices.reshape(16, 2, mesh.shape["tp"]), ("ep_0", "ep_1", "tp"))
    return jax.shard_map(
        shards,
        mesh=torus,
        in_specs=(
            P(EP, "tp"),
            P(EP, "tp"),
            P(EP, "tp"),
            P(),
            P(),
            P(),
            P(None, "tp"),
            P(EP, "tp"),
            P(),
            P(EP, None),
            P(EP, None),
            P(EP, None, "tp"),
            P(EP, None, "tp"),
            P(EP, None, "tp"),
        ),
        out_specs=(P(EP, "tp"), P(EP, "tp")),
        check_vma=False,
    )
```

profile of v0, /device:TPU:1, one launch (start us, length us, event | category | flops | bytes accessed | tf_op | source)
XLA Modules:
  0.0 310.1 jit_solution(1185379400146651329)
XLA Ops:
  7.2 0.9 fusion.50
  8.1 0.8 fusion.51
  9.4 1.4 pad_maximum_fusion.1
  10.8 0.8 copy.42
  11.9 0.7 broadcast_multiply_fusion.2
  12.9 1.2 reduce-window.6
  14.1 0.2 slice_reduce_fusion
  14.3 0.9 concatenate.47
  15.4 2.4 scatter_custom_fusion
  17.9 2.8 gather_fusion
  20.9 10.5 %all_to_all.15 = bf16[16,2,1,22,256]{4,0,3,2,1:T(8,128)(2,1)S(1)} all-to-all(bf16[16,2,1,22,256]{4,0,3,2,1:T(8,128)(2,1)S(1)} %copy.45), channel_id=1, replica_groups=mesh['ep_0'=16,'ep_1'=2,'tp'=16] {'ep_1'}, dimensions={1} | all-to-all | bytes 720896 | tf_op jit(solution)/shard_map/all_to_all | solution.py:42
  31.4 1.1 copy.46
  32.5 9.6 %all-to-all-start.1 = ((bf16[16,2,1,22,256]{4,1,3,2,0:T(2,128)(2,1)}), bf16[16,2,1,22,256]{4,1,3,2,0:T(2,128)(2,1)S(1)}, u32[]{:S(2)}, u32[]{:S(2)}) async-start(bf16[16,2,1,22,256]{4,1,3,2,0:T(2,128)(2,1)} %copy.46), calls=%async_computation.1 | async-start | bytes 720896 | tf_op jit(solution)/shard_map/all_to_all | solution.py:42
  42.8 0.2 subtract_convert_fusion
  43.2 20.0 %all-to-all-done.1 = bf16[16,2,1,22,256]{4,1,3,2,0:T(2,128)(2,1)S(1)} async-done(((bf16[16,2,1,22,256]{4,1,3,2,0:T(2,128)(2,1)}), bf16[16,2,1,22,256]{4,1,3,2,0:T(2,128)(2,1)S(1)}, u32[]{:S(2)}, u32[]{:S(2)}) %all-to-all-start.1) | async-done | bytes 360480 | tf_op jit(solution)/shard_map/all_to_all | solution.py:42
  63.2 0.8 reshape_reshape_reshape.7
  64.0 0.2 all-gather.8.cloned.1.call-start
  64.3 35.3 %all-gather.4.cloned.1.call-done = bf16[8192,128]{0,1:T(8,128)(2,1)} async-done(((bf16[256,128]{0,1:T(8,128)(2,1)}), bf16[8192,128]{0,1:T(8,128)(2,1)}) %all-gather.4.cloned.1.call-update) | async-done | bytes 2097168 | tf_op jit(solution)/shard_map/all_gather | solution.py:23
  99.5 1.7 fusion.70
  101.2 0.6 copy.54
  101.8 1.6 copy.39
  103.4 0.6 copy.55
  104.0 1.5 copy.40
  105.5 25.7 %while.15 = (s32[]{:T(128)}, f32[1,2,256]{2,1,0:T(2,128)S(1)}, f32[1,2,256]{2,1,0:T(2,128)S(1)}, f32[256,1,2,64]{0,3,2,1:T(8,128)S(1)}, bf16[8,1024,1,64]{1,3,2,...) while((s32[]{:T(128)}, f32[1,2,256]{2,1,0:T(2,128)S(1)}, ...), condition=%wide.region_5.6_spmd.clone, body=%wide.region_2.5_spmd.clone.sunk | while | flops 138513408 | bytes 6914169 | solution.py:138
  105.5 1.4 bitcast_reduce_fusion.3
  106.9 0.4 fusion.81
  107.3 1.4 fusion.82
  108.7 1.4 bitcast_reduce_fusion.3
  110.1 0.4 fusion.81
  110.5 1.4 fusion.82
  111.9 1.4 bitcast_reduce_fusion.3
  113.4 0.4 fusion.81
  113.7 1.4 fusion.82
  115.2 1.4 bitcast_reduce_fusion.3
  116.6 0.4 fusion.81
  117.0 1.4 fusion.82
  118.4 1.4 bitcast_reduce_fusion.3
  119.8 0.4 fusion.81
  120.2 1.4 fusion.82
  121.6 1.4 bitcast_reduce_fusion.3
  123.0 0.4 fusion.81
  123.4 1.4 fusion.82
  124.8 1.4 bitcast_reduce_fusion.3
  126.2 0.4 fusion.81
  126.6 1.4 fusion.82
  128.0 1.4 bitcast_reduce_fusion.3
  129.4 0.4 fusion.81
  129.8 1.4 fusion.82
  131.4 42.5 %all-gather.6.cloned.1.call-done = bf16[704,4096]{1,0:T(8,128)(2,1)} async-done(((bf16[704,256]{1,0:T(8,128)(2,1)}), bf16[704,4096]{1,0:T(8,128)(2,1)}) %all-gather.6.cloned.1.call-update) | async-done | bytes 5767184 | tf_op jit(solution)/shard_map/all_gather | solution.py:166
  173.9 4.0 %fusion.19 = f32[704]{0:T(1024)S(1)} fusion(bf16[704,4096]{1,0:T(8,128)(2,1)} %all-gather.6.cloned.1.call-done), kind=kLoop, calls=%fused_computation.32 | loop fusion | flops 8650048 | bytes 5769984 | tf_op jit(solution)/shard_map/reduce_sum | solution.py:173
  177.9 0.3 copy-done.1
  178.2 3.0 fusion.31
  181.2 1.7 fusion.40
  182.9 0.7 pad_maximum_fusion
  183.7 70.5 %all-gather.8.cloned.1.call-done = bf16[960,2048]{1,0:T(8,128)(2,1)} async-done(((bf16[960,128]{1,0:T(8,128)(2,1)}), bf16[960,2048]{1,0:T(8,128)(2,1)}) %all-gather.8.cloned.1.call-update) | async-done | bytes 3932176 | tf_op jit(solution)/shard_map/all_gather | solution.py:23
  254.2 2.7 fusion.28
  256.9 0.8 reshape.435
  257.8 14.4 %all-to-all-start.2 = ((bf16[32,22,256]{2,1,0:T(8,128)(2,1)}), bf16[32,22,256]{2,1,0:T(8,128)(2,1)S(1)}, u32[]{:S(2)}, u32[]{:S(2)}) async-start(bf16[32,22,256]{2,1,0:T(8,128)(2,1)} %reshape.435), calls=%async_computation.2 | async-start | bytes 786432 | tf_op jit(solution)/shard_map/all_to_all | solution.py:191
  272.3 1.5 fusion.27
  273.8 2.3 fusion.43
  276.2 23.7 %all-to-all-done.2 = bf16[32,22,256]{2,1,0:T(8,128)(2,1)S(1)} async-done(((bf16[32,22,256]{2,1,0:T(8,128)(2,1)}), bf16[32,22,256]{2,1,0:T(8,128)(2,1)S(1)}, u32[]{:S(2)}, u32[]{:S(2)}) %all-to-all-start.2) | async-done | bytes 360480 | tf_op jit(solution)/shard_map/all_to_all | solution.py:191
  300.0 2.0 gather_fusion.1
  301.9 0.3 reshape.437
  302.2 1.4 multiply_reduce_fusion
  (90 shorter events, 3.0 us)
Async XLA Ops:
  7.2 247.0 %copy-start = (bf16[1,2048,256]{2,1,0:T(8,128)(2,1)S(1)}, bf16[1,2048,256]{2,1,0:T(8,128)(2,1)}, u32[]{:S(2)}) copy-start(bf16[1,2048,256]{2,1,0:T(8,128)(2,1)} %param.29) | copy-start | bytes 3145732
  7.2 92.3 %all-gather.4.cloned.1.call-start = ((), (), s32[]{:S(2)}) async-start(), calls=%async_computation.3 | async-start | bytes 2162688 | tf_op jit(solution)/shard_map/all_gather | solution.py:23
  17.9 24.3 %copy-start.2 = (bf16[256,128]{1,0:T(8,128)(2,1)S(1)}, bf16[256,128]{1,0:T(8,128)(2,1)}, u32[]{:S(2)}) copy-start(bf16[256,128]{1,0:T(8,128)(2,1)} %param.16) | copy-start | bytes 196612
  17.9 24.5 %copy-start.4 = (f32[64]{0:T(128)S(1)}, f32[64]{0:T(128)}, u32[]{:S(2)}) copy-start(f32[64]{0:T(128)} %param.19) | copy-start | bytes 772
  32.5 30.6 %all-to-all-start.1 = ((bf16[16,2,1,22,256]{4,1,3,2,0:T(2,128)(2,1)}), bf16[16,2,1,22,256]{4,1,3,2,0:T(2,128)(2,1)S(1)}, u32[]{:S(2)}, u32[]{:S(2)}) async-start(bf16[16,2,1,22,256]{4,1,3,2,0:T(2,128)(2,1)} %copy.46), calls=%async_computation.1 | async-start | bytes 720896 | tf_op jit(solution)/shard_map/all_to_all | solution.py:42
  42.1 131.8 %all-gather.6.cloned.1.call-start = ((), (), s32[]{:S(2)}) async-start(), calls=%async_computation.4 | async-start | bytes 6127616 | tf_op jit(solution)/shard_map/all_gather | solution.py:166
  64.0 190.1 %all-gather.8.cloned.1.call-start = ((), (), s32[]{:S(2)}) async-start(), calls=%async_computation.5 | async-start | bytes 4177920 | tf_op jit(solution)/shard_map/all_gather | solution.py:23
  131.2 46.7 %copy-start.7 = (f32[4096]{0:T(1024)S(1)}, f32[4096]{0:T(1024)}, u32[]{:S(2)}) copy-start(f32[4096]{0:T(1024)} %param.24) | copy-start | bytes 49156
  173.9 4.3 %copy-start.1 = (bf16[704,4096]{1,0:T(8,128)(2,1)S(1)}, bf16[704,4096]{1,0:T(8,128)(2,1)}, u32[]{:S(2)}) copy-start(bf16[704,4096]{1,0:T(8,128)(2,1)} %all-gather.6.cloned.1.call-done) | copy-start | bytes 17301508
  178.2 3.0 copy-start.5
  183.7 88.5 %copy-start.3 = (f32[256,2]{0,1:T(2,128)S(1)}, f32[256,2]{0,1:T(2,128)}, u32[]{:S(2)}) copy-start(f32[256,2]{0,1:T(2,128)} %param.26) | copy-start | bytes 6148
  183.7 90.1 %copy-start.6 = (bf16[2048,256]{1,0:T(8,128)(2,1)S(1)}, bf16[2048,256]{1,0:T(8,128)(2,1)}, u32[]{:S(2)}) copy-start(bf16[2048,256]{1,0:T(8,128)(2,1)} %param.22) | copy-start | bytes 3145732
  183.7 90.1 %copy-start.8 = (f32[2048]{0:T(1024)S(1)}, f32[2048]{0:T(1024)}, u32[]{:S(2)}) copy-start(f32[2048]{0:T(1024)} %param.21) | copy-start | bytes 24580
  257.8 42.1 %all-to-all-start.2 = ((bf16[32,22,256]{2,1,0:T(8,128)(2,1)}), bf16[32,22,256]{2,1,0:T(8,128)(2,1)S(1)}, u32[]{:S(2)}, u32[]{:S(2)}) async-start(bf16[32,22,256]{2,1,0:T(8,128)(2,1)} %reshape.435), calls=%async_computation.2 | async-start | bytes 786432 | tf_op jit(solution)/shard_map/all_to_all | solution.py:191
Sparse Core Ops, SparseCore 0:
  10.9 88.5 all-gather.3
  102.5 71.3 all-gather.5
  183.8 70.3 all-gather.7
where the time goes:
time: 311 us; the launch traced here: 310 us
  waiting for transfers between devices  192 us (62%)
  matrix products  31.9 us (10%)
  starting transfers between devices  24.3 us (8%)
  local copies, waits for them, and re-layouts  20.2 us (6%)
  other arithmetic  16.7 us (5%)
  between operations  14.2 us (5%)
  blocking collectives  10.5 us (3%)
    all_gather x2, waiting for transfers between devices, in_one_piece(): filled = lax.all_gather(both, axis, axis=dim, tiled=True)  106 us
    all_gather x1, waiting for transfers between devices, shards(): lax.all_gather(arrived, 'tp', axis=1, tiled=True).astype(jnp.float32)  42.5 us
    all_to_all x1, waiting for transfers between devices, shards(): lax.all_to_all(expert_back, EP, split_axis=0, concat_axis=0, tiled=True)  23.7 us
    all_to_all x1, waiting for transfers between devices, exchange_in_order(): filled = lax.all_to_all(filled, axes[k], k, k, tiled=True)  20 us
    all_to_all x1, starting transfers between devices, shards(): lax.all_to_all(expert_back, EP, split_axis=0, concat_axis=0, tiled=True)  14.4 us
    dot_general x8, matrix products, absorb(): jnp.einsum('hgrn,nhd->rhgd', rounded, value_block, preferred_element_type...  11.1 us
    dot_general x8, matrix products, absorb(): jnp.einsum('rhgd,nhd->hgrn', query_heads, key_block, preferred_element_ty...  11 us
    all_to_all x1, blocking collectives, exchange_in_order(): filled = lax.all_to_all(filled, axes[k], k, k, tiled=True)  10.5 us
  transfers between devices with their start and end apart: 5, of which 5 were waited for; matrix products, arithmetic and copies ran while one was open for 16% of the time, Pallas kernels for 0%

commit v1 on v0

v1 whole, which is shorter than its diff:
```python
import functools

import jax
import jax.numpy as jnp
import numpy as np
from jax import lax
from jax.experimental import pallas as pl
from jax.experimental.pallas import tpu as pltpu
from jax.sharding import Mesh
from jax.sharding import PartitionSpec as P

MESH = pl.DeviceIdType.MESH
EP = ("z", "c")
TP = ("y", "x")
HEAD = 64
GRID_W = 64
EPS = 1e-06
THETA = 10000.0
NZ = 16
NX = 4
TOK = 256
CAP = 22
PAD = 24
EXPERTS = 32
D = 4096
QDIM = 2048

OFFSETS = ((0, 1), (-1, 2), (3, -4), (5, -5), (6, -6), (7, -7), (8, 4), (-2, -3))
CHUNKS = len(OFFSETS)
BLOCKS = [(dz, dc) for part in OFFSETS for dz in part for dc in (0, 1)]
SPANS = [(2 * sum(map(len, OFFSETS[:n])), 2 * len(OFFSETS[n])) for n in range(CHUNKS)]
MOST = PAD * max(count for begin, count in SPANS)

ORDER = (
    "S1", "S0", "S7", "S5", "S6", "A1", "A0", "A7", "X11", "Q", "K0", "X01", "X12", "X02", "X71", "X72", "S2", "X13",
    "X04", "A5", "X03", "S3", "X73", "X74", "X14", "K1", "S4", "A6", "T0", "X51", "A2", "X05", "X75", "T1", "X15",
    "X52", "K2", "X61", "X53", "A3", "X21", "X62", "L0", "L1", "E7", "X22", "K3", "X63", "T2", "X54", "A4", "X55",
    "X31", "X23", "K4", "X65", "X64", "T3", "X41", "X42", "T4", "E5", "K5", "X24", "X33", "E6", "X43", "X44", "X25",
    "T5", "H51", "X34", "K6", "E1", "X45", "H61", "X35", "X32", "T6", "H53", "H72", "H54", "H71", "E2", "H52", "E4",
    "K7", "H55", "H64", "H63", "H11", "E3", "H73", "E0", "H41", "L2", "J5", "H42", "K8", "H62", "H65", "H21", "H74",
    "T7", "H75", "H31", "T8", "H43", "H13", "H44", "M0", "H12", "J6", "J7", "H34", "H33", "H23", "H45", "H22", "H15",
    "H01", "H32", "M2", "H02", "H35", "M1", "H24", "J4", "H04", "H14", "H25", "H03", "J3", "M4", "M3", "H05", "J2",
    "J1", "M5", "J0", "L3", "M6", "R",
)


def angle_tables():
    half = HEAD // 2
    inverse = (np.float32(THETA) ** (-np.arange(0, half, 2, dtype=np.float32) / np.float32(half))).astype(np.float32)
    angles = (np.arange(128, dtype=np.float32)[:, None] * inverse).astype(np.float32).astype(np.float64)
    pair = np.repeat(np.stack([np.cos(angles), np.sin(angles)]), 2, axis=2).astype(np.float32)
    pair[1, :, 0::2] *= -1
    none = np.zeros_like(pair)
    by_row = np.concatenate([pair, none, pair, none], axis=2)
    by_col = np.concatenate([none, pair, none, pair], axis=2)[:, :GRID_W]
    return by_row, by_col


def wrap(a, n):
    return lax.rem(a + n, n)


def norm_turn(x, gain, cosine, sine):
    low = lax.broadcasted_iota(jnp.int32, x.shape, 1) < HEAD
    squares = x * x
    first = jnp.sum(jnp.where(low, squares, 0.0), axis=1, keepdims=True)
    second = jnp.sum(jnp.where(low, 0.0, squares), axis=1, keepdims=True)
    x = x * lax.rsqrt(jnp.where(low, first, second) / HEAD + EPS) * gain
    even = lax.rem(lax.broadcasted_iota(jnp.int32, x.shape, 1), 2) == 0
    other = jnp.where(even, pltpu.roll(x, 127, 1), pltpu.roll(x, 1, 1))
    return x * cosine + other * sine


def dot(a, b, dims=((1,), (0,))):
    return lax.dot_general(a, b, (dims, ((), ())), preferred_element_type=jnp.float32)


def kernel(
    *refs,
):
    sources, (wo_hbm, wg_hbm, wu_hbm, wd_hbm) = refs[:12], refs[12:16]
    (att_ref, mix_ref), held = refs[16:18], refs[18:30]
    (
        gains, cs, q1, q2, kv, run_max, run_sum, run_acc, pick, out, xs, hs, ho, back, ret, acc, sq, wgu, wd, wo,
        sent, disp_r, ret_r, ag_r, kz_r, kd_r, w_s, own_s, in_s,
    ) = refs[30:]
    ids_ref, x_ref, q_ref, kt_ref, vt_ref, qg_ref, kg_ref, byrow_ref, bycol_ref, mg_ref, eg_ref, rw_ref = held
    z, c = lax.axis_index("z"), lax.axis_index("c")
    y, x = lax.axis_index("y"), lax.axis_index("x")
    coord = {"y": y, "x": x}

    barrier = pltpu.get_barrier_semaphore()

    def partner(dz, dc):
        return {"z": lax.rem(z + (dz + NZ), NZ), "c": lax.rem(c + dc, 2)}

    def side(axis, step):
        return {axis: lax.rem(coord[axis] + (step + NX), NX)}

    for dz, dc in BLOCKS[1:]:
        pl.semaphore_signal(barrier, inc=1, device_id=partner(dz, dc), device_id_type=MESH)
    for axis in ("x", "y"):
        for step in (1, -1):
            pl.semaphore_signal(barrier, inc=1, device_id=side(axis, step), device_id_type=MESH)

    inputs = [pltpu.make_async_copy(src, dst, in_s.at[k]) for k, (src, dst) in enumerate(zip(sources, held))]
    for load in inputs:
        load.start()
    loads = [
        pltpu.make_async_copy(wg_hbm.at[0], wgu.at[:, 0:128], w_s.at[0]),
        pltpu.make_async_copy(wu_hbm.at[0], wgu.at[:, 128:256], w_s.at[1]),
        pltpu.make_async_copy(wd_hbm.at[0], wd, w_s.at[2]),
        pltpu.make_async_copy(wo_hbm, wo, w_s.at[3]),
    ]

    for load in inputs[:2]:
        load.wait()
    for load in loads:
        load.start()

    experts = lax.broadcasted_iota(jnp.int32, (EXPERTS, TOK), 0)
    hits = [jnp.where(experts == ids_ref[k : k + 1, :], 1.0, 0.0) for k in range(2)]
    earlier = lax.broadcasted_iota(jnp.int32, (TOK, TOK), 0) < lax.broadcasted_iota(jnp.int32, (TOK, TOK), 1)
    before = dot((hits[0] + hits[1]).astype(jnp.bfloat16), jnp.where(earlier, 1.0, 0.0).astype(jnp.bfloat16))
    keys = [
        ids_ref[k : k + 1, :].astype(jnp.float32) * 32.0 + jnp.sum(hits[k] * before, axis=0, keepdims=True)
        for k in range(2)
    ]
    places = lax.broadcasted_iota(jnp.int32, (PAD, TOK), 0)
    for n in range(CHUNKS):
        wanted = []
        begin, count = SPANS[n]
        for dz, dc in BLOCKS[begin : begin + count]:
            to = partner(dz, dc)
            wanted.append((places + (to["z"] * 2 + to["c"]) * 32).astype(jnp.float32))
        wanted = jnp.concatenate(wanted, axis=0)
        rows = pl.ds(begin * PAD, count * PAD)
        marks = [jnp.where(wanted == keys[k], 1.0, 0.0) for k in range(2)]
        for k in range(2):
            pick[k, rows, :] = marks[k].astype(jnp.bfloat16)
        chosen = dot((marks[0] + marks[1]).astype(jnp.bfloat16), x_ref[...])
        for h in range(2):
            out[h, begin : begin + count] = (
                chosen[:, h * 128 : (h + 1) * 128].reshape(count, PAD, 128).astype(jnp.bfloat16)
            )

    pl.semaphore_wait(barrier, len(BLOCKS) - 1 + 4)

    def arrived(ref, sem):
        remote(ref, ref, sem, sem, partner(0, 1)).wait_recv()

    def left(ref, sem):
        remote(ref, ref, sem, sem, partner(0, 1)).wait_send()

    def remote(src, dst, send, recv, device):
        return pltpu.make_async_remote_copy(
            src_ref=src, dst_ref=dst, send_sem=send, recv_sem=recv, device_id=device, device_id_type=MESH
        )

    chunk_of = [n for n, (begin, count) in enumerate(SPANS) for k in range(count)]

    def dispatch(i):
        return remote(out.at[:, i], xs.at[:, 0, 0, i], sent.at[0], disp_r.at[chunk_of[i]], partner(*BLOCKS[i]))

    def giveback(i):
        dz, dc = BLOCKS[i]
        return remote(back.at[i], ret.at[i], sent.at[1], ret_r.at[0], partner(-dz, dc))

    own_out = pltpu.make_async_copy(out.at[:, 0], xs.at[:, 0, 0, 0], own_s.at[0])
    own_back = pltpu.make_async_copy(back.at[0], ret.at[0], own_s.at[1])

    def queries_and_keys():
        for load in inputs[2:]:
            load.wait()
        first_row = (z * 2 + c) * (TOK // GRID_W)
        for g in range(TOK // GRID_W):
            for t in range(2):
                cs[t, g * GRID_W : (g + 1) * GRID_W, :] = byrow_ref[t, pl.ds(first_row + g, 1), :] + bycol_ref[t]
        for t, ref in enumerate((qg_ref, kg_ref)):
            gains[t : t + 1, 0:HEAD] = ref[...]
            gains[t : t + 1, HEAD:128] = ref[...]
        low = lax.broadcasted_iota(jnp.int32, (128, 128), 1) < HEAD
        keys_raw = kt_ref[...].astype(jnp.float32)
        keys_raw = jnp.concatenate([keys_raw[:, 0:128], keys_raw[:, 128:256]], axis=0).T
        kv[0, 0, 0:128, :] = norm_turn(
            keys_raw, gains[1:2, :], jnp.where(low, cs[0, 0:128], cs[0, 128:256]), jnp.where(low, cs[1, 0:128], cs[1, 128:256])
        ).astype(jnp.bfloat16)
        kv[0, 0, 128:192, :] = vt_ref[:, 0:128]
        kv[0, 0, 192:256, :] = vt_ref[:, 128:256]
        turned = norm_turn(q_ref[...].astype(jnp.float32), gains[0:1, :], cs[0], cs[1])
        turned = turned.astype(jnp.bfloat16).astype(jnp.float32) * 0.125
        low = lax.broadcasted_iota(jnp.int32, (TOK, 128), 1) < HEAD
        crossed = pltpu.roll(turned, HEAD, 1)
        q1[0:TOK, :] = jnp.where(low, turned, 0.0).astype(jnp.bfloat16)
        q1[TOK:, :] = jnp.where(low, crossed, 0.0).astype(jnp.bfloat16)
        q2[0:TOK, :] = jnp.where(low, 0.0, crossed).astype(jnp.bfloat16)
        q2[TOK:, :] = jnp.where(low, 0.0, turned).astype(jnp.bfloat16)
        run_max[...] = jnp.full_like(run_max, -jnp.inf)
        run_sum[...] = jnp.zeros_like(run_sum)
        run_acc[...] = jnp.zeros_like(run_acc)

    def stage_s(n):
        for i in range(SPANS[n][0], sum(SPANS[n])):
            if i == 0:
                own_out.start()
            else:
                dispatch(i).start()

    kinds = (0, 0, 1, 1, 2, 2, 3, 3, 5, 5, 4, 4, 5, 5, 5, 5)

    def gather(buf, begin, count, half, index, send):
        inner, outer = ("x", "y") if half == 0 else ("y", "x")
        lo, hi, whole = pl.ds(begin, count // 2), pl.ds(begin + count // 2, count - count // 2), pl.ds(begin, count)

        def at(o, i, part=whole):
            return buf.at[half, o, i, part]

        def copy(k, src, dst, axis, step):
            return remote(src, dst, sent.at[send], ag_r.at[index, kinds[k]], side(axis, step))

        both = pl.ds(1, 2)
        return [
            copy(0, at(0, 0), at(0, 2), inner, 1),
            copy(1, at(0, 0), at(0, 1), inner, -1),
            copy(2, at(0, 0), at(2, 0), outer, 1),
            copy(3, at(0, 0), at(1, 0), outer, -1),
            copy(4, at(0, 2, lo), at(0, 3, lo), inner, 1),
            copy(5, at(0, 1, hi), at(0, 3, hi), inner, -1),
            copy(6, at(0, both), at(2, both), outer, 1),
            copy(7, at(0, both), at(1, both), outer, -1),
            copy(8, at(2, 0, lo), at(3, 0, lo), outer, 1),
            copy(9, at(1, 0, hi), at(3, 0, hi), outer, -1),
            copy(10, at(0, 3), at(2, 3), outer, 1),
            copy(11, at(0, 3), at(1, 3), outer, -1),
            copy(12, at(2, 1), at(3, 1), outer, 1),
            copy(13, at(1, 2), at(3, 2), outer, -1),
            copy(14, at(2, 3, lo), at(3, 3, lo), outer, 1),
            copy(15, at(1, 3, hi), at(3, 3, hi), outer, -1),
        ]

    def both_halves(buf, begin, count, index, send):
        part, middle = pl.ds(begin, count), pl.ds(1, 2)
        landed = (
            buf.at[:, 0, middle, part], buf.at[:, middle, 0, part], buf.at[:, 0, 3, part],
            buf.at[:, middle, middle, part], buf.at[:, middle, 3, part], buf.at[:, 3, :, part],
        )
        return [gather(buf, begin, count, h, index, send) for h in range(2)], landed, index

    gx = [both_halves(xs, *SPANS[n], n, 2) for n in range(CHUNKS)]
    gh = [both_halves(hs, SPANS[n][0] // 2, SPANS[n][1] // 2, CHUNKS + n, 3) for n in range(CHUNKS)]
    gm = both_halves(ho, 0, 128, CHUNKS * 2, 4)

    steps = ((0, 1, 2, 3), (4, 5, 6, 7), (8, 9), (10, 11), (12, 13), (14, 15), ())

    def go(pair, step):
        gathers, landed, index = pair
        if step:
            arrived(landed[step - 1], ag_r.at[index, step - 1])
        for g in gathers:
            for k in steps[step]:
                g[k].start()

    def slots(t):
        ry, rx = (r + r // 2 - 2 * (r // 3) for r in (wrap(t // NX - y, NX), wrap(lax.rem(t, NX) - x, NX)))
        return (ry, rx), (rx, ry)

    def stage_a(n):
        begin, count = SPANS[n]
        if n == 0:
            own_out.wait()
            begin, count = 1, count - 1
        arrived(xs.at[:, 0, 0, pl.ds(begin, count)], disp_r.at[n])
        go(gx[n], 0)

    def feed_forward(n):
        begin, count = SPANS[n]
        rows, part_rows = pl.ds(0, count * PAD), count * PAD // 2
        acc[rows, :] = jnp.zeros((count * PAD, 256), jnp.float32)
        sq[rows, :] = jnp.zeros((count * PAD, 128), jnp.float32)

        def body(g, carry):
            parts, squares = [], None
            for k in range(4):
                t = g * 4 + k
                for h, (o, i) in enumerate(slots(t)):
                    part = xs[h, o, i, begin : begin + count].astype(jnp.float32).reshape(count * PAD, 128)
                    squares = part * part if squares is None else squares + part * part
                    parts.append((part * eg_ref[pl.ds(2 * t + h, 1), :]).astype(jnp.bfloat16))
            sq[rows, :] += squares
            weight = wgu[pl.ds(pl.multiple_of(g * 1024, 1024), 1024), :]
            acc[rows, :] += dot(jnp.concatenate(parts, axis=1), weight)
            return carry

        lax.fori_loop(0, 4, body, 0)
        stat = lax.rsqrt(jnp.sum(sq[rows, :], axis=1, keepdims=True) / D + EPS)
        gate = acc[rows, 0:128] * stat
        up = acc[rows, 128:256] * stat
        hidden = gate / (1.0 + jnp.exp(-gate)) * up
        for h in range(2):
            own = hidden[h * part_rows : (h + 1) * part_rows].reshape(count // 2, PAD, 128)
            hs[h, 0, 0, begin // 2 : (begin + count) // 2] = own.astype(jnp.bfloat16)

    def down(n):
        begin, count = SPANS[n]
        parts = []
        for t in range(16):
            pair = [hs[h, o, i, begin // 2 : (begin + count) // 2] for h, (o, i) in enumerate(slots(t))]
            pair = jnp.concatenate(pair, axis=0).astype(jnp.float32).reshape(count * PAD, 128)
            parts.append(pair.astype(jnp.bfloat16))
        result = dot(jnp.concatenate(parts, axis=1), wd[...])
        back[begin : begin + count] = result.reshape(count, PAD, 256).astype(jnp.bfloat16)
        for i in range(SPANS[n][0], sum(SPANS[n])):
            if i == 0:
                own_back.start()
            else:
                giveback(i).start()

    def along(s):
        up, dn = (NZ - s) % NZ, s
        if s < 7:
            return [
                remote(kv.at[up, 0], kv.at[(NZ - s - 1) % NZ, 0], sent.at[5], kz_r.at[0, s], partner(1, 0)),
                remote(kv.at[dn, 0], kv.at[s + 1, 0], sent.at[5], kz_r.at[1, s], partner(-1, 0)),
            ]
        lo, hi = pl.ds(0, 128), pl.ds(128, 128)
        return [
            remote(kv.at[up, 0, lo], kv.at[8, 0, lo], sent.at[5], kz_r.at[0, s], partner(1, 0)),
            remote(kv.at[dn, 0, hi], kv.at[8, 0, hi], sent.at[5], kz_r.at[1, s], partner(-1, 0)),
        ]

    def across(r):
        return remote(kv.at[r, 0], kv.at[r, 1], sent.at[6], kd_r.at[r], partner(0, 1))

    def absorb(r):
        blocks = kv[r]
        stored = blocks[:, 0:128, :].reshape(256, 128)
        scores = jnp.concatenate(
            [dot(stored, q1[...], ((1,), (1,))), dot(stored, q2[...], ((1,), (1,)))], axis=0
        )
        new_max = jnp.maximum(run_max[...], jnp.max(scores, axis=0, keepdims=True))
        factor = jnp.exp(run_max[...] - new_max)
        raw = jnp.exp(scores - new_max)
        run_sum[...] = run_sum[...] * factor + jnp.sum(raw, axis=0, keepdims=True)
        turned_values = jnp.concatenate(
            [blocks[0, 128:192], blocks[1, 128:192], blocks[0, 192:256], blocks[1, 192:256]], axis=1
        )
        run_acc[...] = run_acc[...] * factor + dot(turned_values, raw.astype(jnp.bfloat16))
        run_max[...] = new_max

    def ring_step(s):
        if s > 0:
            for copy in along(s - 1):
                copy.wait_recv()
        if s < 8:
            for copy in along(s):
                copy.start()
        if 0 < s < 8:
            across(NZ - s).start()
        across(s).start()

    def attend(s):
        across(s).wait_recv()
        if s in (0, 8):
            absorb(s)
        else:
            across(NZ - s).wait_recv()

            def body(k, carry):
                absorb(s + k * (NZ - 2 * s))
                return carry

            lax.fori_loop(0, 2, body, 0)

    def heads():
        result = run_acc[...] / run_sum[...]
        result = jnp.concatenate([result[:, 0:TOK], result[:, TOK:]], axis=0).T.astype(jnp.bfloat16)
        ho[0, 0, 0] = result[0:128]
        ho[1, 0, 0] = result[128:256]

    def mix():
        parts, squares = [], None
        for t in range(16):
            part = jnp.concatenate([ho[h, o, i] for h, (o, i) in enumerate(slots(t))], axis=0).astype(jnp.float32)
            squares = part * part if squares is None else squares + part * part
            parts.append((part * mg_ref[pl.ds(t, 1), :]).astype(jnp.bfloat16))
        total = dot(jnp.concatenate(parts, axis=1), wo[...])
        scale = lax.rsqrt(jnp.sum(squares, axis=1, keepdims=True) / QDIM + EPS)
        att_ref[...] = (total * scale).astype(jnp.bfloat16)

    def combine():
        own_back.wait()
        arrived(ret.at[pl.ds(1, EXPERTS - 1)], ret_r.at[0])
        rows = ret[...].astype(jnp.float32).reshape(EXPERTS * PAD, 256).astype(jnp.bfloat16)
        same = lax.broadcasted_iota(jnp.int32, (TOK, TOK), 0) == lax.broadcasted_iota(jnp.int32, (TOK, TOK), 1)
        total = None
        for k in range(2):
            weight = jnp.sum(jnp.where(same, rw_ref[k : k + 1, :], 0.0), axis=1, keepdims=True)
            term = dot(pick[k], rows, ((0,), (0,))) * weight
            total = term if total is None else total + term
        mix_ref[...] = total.astype(jnp.bfloat16)

    for name in ORDER:
        kind, n, step = name[0], int(name[1:2] or 0), int(name[2:] or 0)
        if kind == "S":
            stage_s(n)
        elif kind == "A":
            stage_a(n)
        elif kind == "X":
            go(gx[n], step)
        elif kind == "E":
            go(gx[n], 6)
            feed_forward(n)
            go(gh[n], 0)
        elif kind == "H":
            go(gh[n], step)
        elif kind == "J":
            go(gh[n], 6)
            down(n)
        elif kind == "K":
            ring_step(n)
        elif kind == "T":
            attend(n)
        elif kind == "M":
            if n == 0:
                heads()
            go(gm, n)
            if n == 6:
                mix()
        elif kind == "Q":
            queries_and_keys()
        elif kind == "L":
            loads[n].wait()
        else:
            combine()

    left(out.at[:, pl.ds(1, EXPERTS - 1)], sent.at[0])
    left(back.at[pl.ds(1, EXPERTS - 1)], sent.at[1])
    left(xs.at[:, :, :, pl.ds(0, 30)], sent.at[2])
    left(hs.at[:, :, :, pl.ds(0, 15)], sent.at[3])
    left(xs.at[:, :, 0, pl.ds(0, 20)], sent.at[4])
    left(kv.at[pl.ds(1, NZ - 1), 0], sent.at[5])
    left(kv.at[:, 0], sent.at[6])


def shards(
    queries, key_rows, values, query_gain, key_gain, mix_gain, out_weight, expert_input, expert_gain, route_ids,
    route_weights, expert_gate, expert_up, expert_down,
):
    by_row, by_col = angle_tables()
    operands = (
        route_ids.T, expert_input, queries, key_rows.T, values.T, query_gain.reshape(1, HEAD), key_gain.reshape(1, HEAD),
        jnp.asarray(by_row), jnp.asarray(by_col), mix_gain.reshape(16, 128), expert_gain.reshape(32, 128),
        route_weights.T, out_weight, expert_gate, expert_up, expert_down,
    )
    vmem = pl.BlockSpec(memory_space=pltpu.VMEM)
    hbm = pl.BlockSpec(memory_space=pl.ANY)
    bf16, f32 = jnp.bfloat16, jnp.float32
    sem = pltpu.SemaphoreType.DMA
    return pl.pallas_call(
        kernel,
        out_shape=(pltpu.VMEM((TOK, 256), bf16), pltpu.VMEM((TOK, 256), bf16)),
        in_specs=[hbm] * 16,
        out_specs=(vmem, vmem),
        scratch_shapes=[
            *(pltpu.VMEM(a.shape, a.dtype) for a in operands[:12]),
            pltpu.VMEM((2, 128), f32),
            pltpu.VMEM((2, TOK, 128), f32),
            pltpu.VMEM((2 * TOK, 128), bf16),
            pltpu.VMEM((2 * TOK, 128), bf16),
            pltpu.VMEM((NZ, 2, 256, 128), bf16),
            pltpu.VMEM((1, 2 * TOK), f32),
            pltpu.VMEM((1, 2 * TOK), f32),
            pltpu.VMEM((HEAD, 2 * TOK), f32),
            pltpu.VMEM((2, EXPERTS * PAD, TOK), bf16),
            pltpu.VMEM((2, EXPERTS, PAD, 128), bf16),
            pltpu.VMEM((2, NX, NX, EXPERTS, PAD, 128), bf16),
            pltpu.VMEM((2, NX, NX, EXPERTS // 2, PAD, 128), bf16),
            pltpu.VMEM((2, NX, NX, 128, 128), bf16),
            pltpu.VMEM((EXPERTS, PAD, 256), bf16),
            pltpu.VMEM((EXPERTS, PAD, 256), bf16),
            pltpu.VMEM((MOST, 256), f32),
            pltpu.VMEM((MOST, 128), f32),
            pltpu.VMEM((D, 256), bf16),
            pltpu.VMEM((QDIM, 256), bf16),
            pltpu.VMEM((QDIM, 256), bf16),
            sem((7,)),
            sem((CHUNKS,)),
            sem((1,)),
            sem((2 * CHUNKS + 1, 6)),
            sem((2, 8)),
            sem((NZ,)),
            sem((4,)),
            sem((2,)),
            sem((12,)),
        ],
        compiler_params=pltpu.CompilerParams(
            collective_id=0, has_side_effects=True, vmem_limit_bytes=60 * 1024 * 1024
        ),
    )(*operands)


def solution(mesh):
    torus = Mesh(mesh.devices.reshape(NZ, 2, NX, NX), EP + TP)
    return jax.shard_map(
        shards,
        mesh=torus,
        in_specs=(
            P(EP, TP), P(EP, TP), P(EP, TP), P(), P(), P(), P(None, TP), P(EP, TP), P(), P(EP, None), P(EP, None),
            P(EP, None, TP), P(EP, None, TP), P(EP, None, TP),
        ),
        out_specs=(P(EP, TP), P(EP, TP)),
        check_vma=False,
    )
```

time: 311 us -> 93 us (0.30)
  waiting for transfers between devices: 192 us -> 0 us
  Pallas kernels: 0 us -> 90.9 us
  matrix products: 31.9 us -> 0 us
  starting transfers between devices: 24.3 us -> 0 us
  local copies, waits for them, and re-layouts: 20.2 us -> 1.31 us
  other arithmetic: 16.7 us -> 0 us
  between operations: 14.2 us -> 0.64 us
  blocking collectives: 10.5 us -> 0 us
    all_gather x3 -> x0, waiting for transfers between devices: 148 us -> none  [the longest x2 106 us: in_one_piece(): filled = lax.all_gather(both, axis, axis=dim, tiled=True)]
    pallas_call x0 -> x1, Pallas kernels: none -> 90.9 us  [shards(): pl.pallas_call(kernel, out_shape=(pltpu.VMEM((TOK, 256), bf16), pltpu.VME...]
    all_to_all x2 -> x0, waiting for transfers between devices: 43.6 us -> none  [the longest x1 23.7 us: shards(): lax.all_to_all(expert_back, EP, split_axis=0, concat_axis=0, tiled=True)]
    dot_general x20 -> x0, matrix products: 31.9 us -> none  [the longest x8 11.1 us: absorb(): jnp.einsum('hgrn,nhd->rhgd', rounded, value_block, preferred_element_type...]
    all_to_all x2 -> x0, starting transfers between devices: 24 us -> none  [the longest x1 14.4 us: shards(): lax.all_to_all(expert_back, EP, split_axis=0, concat_axis=0, tiled=True)]
    reduce_sum x14 -> x0, other arithmetic: 10.8 us -> none  [the longest x1 3.98 us: shards(): square_sum = jnp.sum(piece_float * piece_float, axis=1)]
    all_to_all x1 -> x0, blocking collectives: 10.5 us -> none  [exchange_in_order(): filled = lax.all_to_all(filled, axes[k], k, k, tiled=True)]
    gather x2 -> x0, local copies, waits for them, and re-layouts: 4.77 us -> none  [the longest x1 2.81 us: shards(): outgoing = padded[slot_rows].reshape(experts_count, capacity, width_local)]
  transfers between devices with their start and end apart: 5 -> 0, of which waited for: 5 -> 0; matrix products, arithmetic and copies ran while one was open for 16% -> 0% of each run, Pallas kernels for 0% -> 0%
where the time goes in v1:
time: 93 us; the launch traced here: 92.9 us
  Pallas kernels  90.9 us (98%)
  local copies, waits for them, and re-layouts  1.31 us (1%)
    pallas_call x1, Pallas kernels, shards(): pl.pallas_call(kernel, out_shape=(pltpu.VMEM((TOK, 256), bf16), pltpu.VME...  90.9 us

profile of v1, /device:TPU:1, one launch (start us, length us, event | category | flops | bytes accessed | tf_op | source)
XLA Modules:
  0.0 92.9 jit_solution(2929482592243559857)
XLA Ops:
  0.6 90.9 %shard_map.167 = (bf16[256,256]{1,0:T(8,128)(2,1)S(1)}, bf16[256,256]{1,0:T(8,128)(2,1)S(1)}) custom-call(s32[2,256]{1,0:T(2,128)} %bitcast.12, bf16[256,256]{1,0:T(8,128)(2,1)} %refs_1_.1, bf16[256,128]{1,0:T(8,128)(2,1)} %refs_2_.1, bf16[64,256]{1,0:T(8,128)(2,1)} %bitcast.8, bf16[64,256]{1,0:T(8,128)(2,1)} %bitcast.9, f32[1,64]{1,0:T(1,128)} %bitcast.14, ...), custom_call_target="tpu_custom_call" | custom-call | tf_op jit(solution)/shard_map/pallas_call | solution.py:459
  91.6 0.7 copy.20
  92.2 0.7 copy.21

commit v2 on v1

--- a/solution.py
+++ b/solution.py
@@ -25,22 +25,26 @@
 D = 4096
 QDIM = 2048
 
-OFFSETS = ((0, 1), (-1, 2), (3, -4), (5, -5), (6, -6), (7, -7), (8, 4), (-2, -3))
+OFFSETS = ((0, 1), (-1, 2), (3, -3), (4, -4), (5, -5), (6, -6), (7, -7), (8, -2))
 CHUNKS = len(OFFSETS)
 BLOCKS = [(dz, dc) for part in OFFSETS for dz in part for dc in (0, 1)]
 SPANS = [(2 * sum(map(len, OFFSETS[:n])), 2 * len(OFFSETS[n])) for n in range(CHUNKS)]
-MOST = PAD * max(count for begin, count in SPANS)
+
+BLOCKS_PER = 4
+ROWS = BLOCKS_PER * CAP
+TILES = ROWS // 8
+HALF = (TILES + 1) // 2
 
 ORDER = (
-    "S1", "S0", "S7", "S5", "S6", "A1", "A0", "A7", "X11", "Q", "K0", "X01", "X12", "X02", "X71", "X72", "S2", "X13",
-    "X04", "A5", "X03", "S3", "X73", "X74", "X14", "K1", "S4", "A6", "T0", "X51", "A2", "X05", "X75", "T1", "X15",
-    "X52", "K2", "X61", "X53", "A3", "X21", "X62", "L0", "L1", "E7", "X22", "K3", "X63", "T2", "X54", "A4", "X55",
-    "X31", "X23", "K4", "X65", "X64", "T3", "X41", "X42", "T4", "E5", "K5", "X24", "X33", "E6", "X43", "X44", "X25",
-    "T5", "H51", "X34", "K6", "E1", "X45", "H61", "X35", "X32", "T6", "H53", "H72", "H54", "H71", "E2", "H52", "E4",
-    "K7", "H55", "H64", "H63", "H11", "E3", "H73", "E0", "H41", "L2", "J5", "H42", "K8", "H62", "H65", "H21", "H74",
-    "T7", "H75", "H31", "T8", "H43", "H13", "H44", "M0", "H12", "J6", "J7", "H34", "H33", "H23", "H45", "H22", "H15",
-    "H01", "H32", "M2", "H02", "H35", "M1", "H24", "J4", "H04", "H14", "H25", "H03", "J3", "M4", "M3", "H05", "J2",
-    "J1", "M5", "J0", "L3", "M6", "R",
+    "S0", "S1", "S2", "S3", "Q", "A0", "S5", "S6", "A1", "X02", "A2", "X01", "X11", "K0", "A3", "S7", "X21", "X03",
+    "X04", "T0", "A5", "K1", "X14", "X13", "X31", "S4", "X05", "X32", "A6", "X51", "X12", "K2", "X33", "X52", "X15",
+    "X34", "X61", "X53", "A7", "K3", "X23", "X35", "A4", "X63", "X54", "X62", "X55", "X71", "T1", "K4", "L0", "L1",
+    "E3", "X41", "T2", "X65", "E5", "X73", "X64", "H31", "K5", "X22", "X72", "T3", "X43", "X74", "T4", "X75", "H51",
+    "X44", "E6", "X25", "X24", "X42", "E1", "K6", "X45", "T5", "H33", "E7", "H32", "H53", "H61", "H34", "E0", "E2",
+    "K7", "E4", "H35", "H71", "T6", "H52", "H55", "H63", "H54", "H64", "T7", "H11", "K8", "H21", "H41", "L2", "J3",
+    "H73", "H62", "T8", "H65", "M0", "J5", "H72", "H74", "H12", "H13", "H43", "H44", "H75", "H24", "H01", "H14",
+    "H42", "J6", "H23", "M1", "H45", "J7", "H03", "H22", "M2", "H15", "H25", "M3", "M4", "H02", "J4", "H04", "H05",
+    "J2", "M5", "J1", "J0", "L3", "M6", "R",
 )
 
 
@@ -81,7 +85,7 @@
     sources, (wo_hbm, wg_hbm, wu_hbm, wd_hbm) = refs[:12], refs[12:16]
     (att_ref, mix_ref), held = refs[16:18], refs[18:30]
     (
-        gains, cs, q1, q2, kv, run_max, run_sum, run_acc, pick, out, xs, hs, ho, back, ret, acc, sq, wgu, wd, wo,
+        gains, cs, q1, q2, kv, run_max, run_sum, run_acc, pick, out, land, xs, hs, ho, back, ret, wgu, wd, wo,
         sent, disp_r, ret_r, ag_r, kz_r, kd_r, w_s, own_s, in_s,
     ) = refs[30:]
     ids_ref, x_ref, q_ref, kt_ref, vt_ref, qg_ref, kg_ref, byrow_ref, bycol_ref, mg_ref, eg_ref, rw_ref = held
@@ -97,7 +101,7 @@
     def side(axis, step):
         return {axis: lax.rem(coord[axis] + (step + NX), NX)}
 
-    for dz, dc in BLOCKS[1:]:
+    for dz, dc in sorted(BLOCKS[1:], key=lambda block: -abs(block[0])):
         pl.semaphore_signal(barrier, inc=1, device_id=partner(dz, dc), device_id_type=MESH)
     for axis in ("x", "y"):
         for step in (1, -1):
@@ -160,13 +164,13 @@
     chunk_of = [n for n, (begin, count) in enumerate(SPANS) for k in range(count)]
 
     def dispatch(i):
-        return remote(out.at[:, i], xs.at[:, 0, 0, i], sent.at[0], disp_r.at[chunk_of[i]], partner(*BLOCKS[i]))
+        return remote(out.at[:, i], land.at[:, i], sent.at[0], disp_r.at[chunk_of[i]], partner(*BLOCKS[i]))
 
     def giveback(i):
         dz, dc = BLOCKS[i]
         return remote(back.at[i], ret.at[i], sent.at[1], ret_r.at[0], partner(-dz, dc))
 
-    own_out = pltpu.make_async_copy(out.at[:, 0], xs.at[:, 0, 0, 0], own_s.at[0])
+    own_out = pltpu.make_async_copy(out.at[:, 0], land.at[:, 0], own_s.at[0])
     own_back = pltpu.make_async_copy(back.at[0], ret.at[0], own_s.at[1])
 
     def queries_and_keys():
@@ -216,7 +220,7 @@
             return buf.at[half, o, i, part]
 
         def copy(k, src, dst, axis, step):
-            return remote(src, dst, sent.at[send], ag_r.at[index, kinds[k]], side(axis, step))
+            return remote(src, dst, sent.at[send + (k in (4, 5, 8, 9, 14, 15))], ag_r.at[index, kinds[k]], side(axis, step))
 
         both = pl.ds(1, 2)
         return [
@@ -246,9 +250,9 @@
         )
         return [gather(buf, begin, count, h, index, send) for h in range(2)], landed, index
 
-    gx = [both_halves(xs, *SPANS[n], n, 2) for n in range(CHUNKS)]
-    gh = [both_halves(hs, SPANS[n][0] // 2, SPANS[n][1] // 2, CHUNKS + n, 3) for n in range(CHUNKS)]
-    gm = both_halves(ho, 0, 128, CHUNKS * 2, 4)
+    gx = [both_halves(xs, n * TILES, TILES, n, 2) for n in range(CHUNKS)]
+    gh = [both_halves(hs, n * HALF, HALF, CHUNKS + n, 4) for n in range(CHUNKS)]
+    gm = both_halves(ho, 0, 128, CHUNKS * 2, 6)
 
     steps = ((0, 1, 2, 3), (4, 5, 6, 7), (8, 9), (10, 11), (12, 13), (14, 15), ())
 
@@ -269,46 +273,40 @@
         if n == 0:
             own_out.wait()
             begin, count = 1, count - 1
-        arrived(xs.at[:, 0, 0, pl.ds(begin, count)], disp_r.at[n])
+        arrived(land.at[:, pl.ds(begin, count)], disp_r.at[n])
+        for h in range(2):
+            rows = [land[h, SPANS[n][0] + b].astype(jnp.float32)[0:CAP] for b in range(BLOCKS_PER)]
+            rows = jnp.concatenate(rows, axis=0).reshape(TILES, 8, 128)
+            xs[h, 0, 0, n * TILES : (n + 1) * TILES] = rows.astype(jnp.bfloat16)
         go(gx[n], 0)
 
     def feed_forward(n):
-        begin, count = SPANS[n]
-        rows, part_rows = pl.ds(0, count * PAD), count * PAD // 2
-        acc[rows, :] = jnp.zeros((count * PAD, 256), jnp.float32)
-        sq[rows, :] = jnp.zeros((count * PAD, 128), jnp.float32)
-
-        def body(g, carry):
-            parts, squares = [], None
-            for k in range(4):
-                t = g * 4 + k
-                for h, (o, i) in enumerate(slots(t)):
-                    part = xs[h, o, i, begin : begin + count].astype(jnp.float32).reshape(count * PAD, 128)
-                    squares = part * part if squares is None else squares + part * part
-                    parts.append((part * eg_ref[pl.ds(2 * t + h, 1), :]).astype(jnp.bfloat16))
-            sq[rows, :] += squares
-            weight = wgu[pl.ds(pl.multiple_of(g * 1024, 1024), 1024), :]
-            acc[rows, :] += dot(jnp.concatenate(parts, axis=1), weight)
-            return carry
-
-        lax.fori_loop(0, 4, body, 0)
-        stat = lax.rsqrt(jnp.sum(sq[rows, :], axis=1, keepdims=True) / D + EPS)
-        gate = acc[rows, 0:128] * stat
-        up = acc[rows, 128:256] * stat
+        parts, squares = [], None
+        for t in range(16):
+            for h, (o, i) in enumerate(slots(t)):
+                part = xs[h, o, i, n * TILES : (n + 1) * TILES].astype(jnp.float32).reshape(ROWS, 128)
+                squares = part * part if squares is None else squares + part * part
+                parts.append((part * eg_ref[2 * t + h : 2 * t + h + 1, :]).astype(jnp.bfloat16))
+        total = dot(jnp.concatenate(parts, axis=1), wgu[...])
+        stat = lax.rsqrt(jnp.sum(squares, axis=1, keepdims=True) / D + EPS)
+        gate = total[:, 0:128] * stat
+        up = total[:, 128:256] * stat
         hidden = gate / (1.0 + jnp.exp(-gate)) * up
         for h in range(2):
-            own = hidden[h * part_rows : (h + 1) * part_rows].reshape(count // 2, PAD, 128)
-            hs[h, 0, 0, begin // 2 : (begin + count) // 2] = own.astype(jnp.bfloat16)
+            own = hidden[h * (ROWS - HALF * 8) :][0 : HALF * 8].reshape(HALF, 8, 128)
+            hs[h, 0, 0, n * HALF : (n + 1) * HALF] = own.astype(jnp.bfloat16)
 
     def down(n):
         begin, count = SPANS[n]
         parts = []
         for t in range(16):
-            pair = [hs[h, o, i, begin // 2 : (begin + count) // 2] for h, (o, i) in enumerate(slots(t))]
-            pair = jnp.concatenate(pair, axis=0).astype(jnp.float32).reshape(count * PAD, 128)
+            pair = [hs[h, o, i, n * HALF + h : (n + 1) * HALF] for h, (o, i) in enumerate(slots(t))]
+            pair = jnp.concatenate(pair, axis=0).astype(jnp.float32).reshape(ROWS, 128)
             parts.append(pair.astype(jnp.bfloat16))
         result = dot(jnp.concatenate(parts, axis=1), wd[...])
-        back[begin : begin + count] = result.reshape(count, PAD, 256).astype(jnp.bfloat16)
+        none = jnp.zeros((PAD - CAP, 256), jnp.float32)
+        rows = [r for b in range(BLOCKS_PER) for r in (result[b * CAP : (b + 1) * CAP], none)]
+        back[begin : begin + count] = jnp.concatenate(rows, axis=0).reshape(count, PAD, 256).astype(jnp.bfloat16)
         for i in range(SPANS[n][0], sum(SPANS[n])):
             if i == 0:
                 own_back.start()
@@ -319,21 +317,21 @@
         up, dn = (NZ - s) % NZ, s
         if s < 7:
             return [
-                remote(kv.at[up, 0], kv.at[(NZ - s - 1) % NZ, 0], sent.at[5], kz_r.at[0, s], partner(1, 0)),
-                remote(kv.at[dn, 0], kv.at[s + 1, 0], sent.at[5], kz_r.at[1, s], partner(-1, 0)),
+                remote(kv.at[up, 0], kv.at[(NZ - s - 1) % NZ, 0], sent.at[8], kz_r.at[0, s], partner(1, 0)),
+                remote(kv.at[dn, 0], kv.at[s + 1, 0], sent.at[8], kz_r.at[1, s], partner(-1, 0)),
             ]
         lo, hi = pl.ds(0, 128), pl.ds(128, 128)
         return [
-            remote(kv.at[up, 0, lo], kv.at[8, 0, lo], sent.at[5], kz_r.at[0, s], partner(1, 0)),
-            remote(kv.at[dn, 0, hi], kv.at[8, 0, hi], sent.at[5], kz_r.at[1, s], partner(-1, 0)),
+            remote(kv.at[up, 0, lo], kv.at[8, 0, lo], sent.at[8], kz_r.at[0, s], partner(1, 0)),
+            remote(kv.at[dn, 0, hi], kv.at[8, 0, hi], sent.at[8], kz_r.at[1, s], partner(-1, 0)),
         ]
 
     def across(r):
-        return remote(kv.at[r, 0], kv.at[r, 1], sent.at[6], kd_r.at[r], partner(0, 1))
-
-    def absorb(r):
-        blocks = kv[r]
-        stored = blocks[:, 0:128, :].reshape(256, 128)
+        return remote(kv.at[r, 0], kv.at[r, 1], sent.at[9], kd_r.at[r], partner(0, 1))
+
+    def absorb(rs):
+        pairs = [(r, core) for r in rs for core in range(2)]
+        stored = jnp.concatenate([kv[r, core, 0:128, :] for r, core in pairs], axis=0)
         scores = jnp.concatenate(
             [dot(stored, q1[...], ((1,), (1,))), dot(stored, q2[...], ((1,), (1,)))], axis=0
         )
@@ -342,7 +340,7 @@
         raw = jnp.exp(scores - new_max)
         run_sum[...] = run_sum[...] * factor + jnp.sum(raw, axis=0, keepdims=True)
         turned_values = jnp.concatenate(
-            [blocks[0, 128:192], blocks[1, 128:192], blocks[0, 192:256], blocks[1, 192:256]], axis=1
+            [kv[r, core, first : first + HEAD, :] for first in (128, 192) for r, core in pairs], axis=1
         )
         run_acc[...] = run_acc[...] * factor + dot(turned_values, raw.astype(jnp.bfloat16))
         run_max[...] = new_max
@@ -359,17 +357,10 @@
         across(s).start()
 
     def attend(s):
-        across(s).wait_recv()
-        if s in (0, 8):
-            absorb(s)
-        else:
-            across(NZ - s).wait_recv()
-
-            def body(k, carry):
-                absorb(s + k * (NZ - 2 * s))
-                return carry
-
-            lax.fori_loop(0, 2, body, 0)
+        rs = (s,) if s in (0, 8) else (s, NZ - s)
+        for r in rs:
+            across(r).wait_recv()
+        absorb(rs)
 
     def heads():
         result = run_acc[...] / run_sum[...]
@@ -435,11 +426,11 @@
 
     left(out.at[:, pl.ds(1, EXPERTS - 1)], sent.at[0])
     left(back.at[pl.ds(1, EXPERTS - 1)], sent.at[1])
-    left(xs.at[:, :, :, pl.ds(0, 30)], sent.at[2])
-    left(hs.at[:, :, :, pl.ds(0, 15)], sent.at[3])
-    left(xs.at[:, :, 0, pl.ds(0, 20)], sent.at[4])
-    left(kv.at[pl.ds(1, NZ - 1), 0], sent.at[5])
-    left(kv.at[:, 0], sent.at[6])
+    for k, buf in enumerate((xs, hs, ho)):
+        left(buf.at[:, pl.ds(0, 3)], sent.at[2 + 2 * k])
+        left(buf.at[:, 0, pl.ds(0, 3)], sent.at[3 + 2 * k])
+    left(kv.at[pl.ds(1, NZ - 1), 0], sent.at[8])
+    left(kv.at[:, 0], sent.at[9])
 
 
 def shards(
@@ -473,17 +464,16 @@
             pltpu.VMEM((HEAD, 2 * TOK), f32),
             pltpu.VMEM((2, EXPERTS * PAD, TOK), bf16),
             pltpu.VMEM((2, EXPERTS, PAD, 128), bf16),
-            pltpu.VMEM((2, NX, NX, EXPERTS, PAD, 128), bf16),
-            pltpu.VMEM((2, NX, NX, EXPERTS // 2, PAD, 128), bf16),
+            pltpu.VMEM((2, EXPERTS, PAD, 128), bf16),
+            pltpu.VMEM((2, NX, NX, CHUNKS * TILES, 8, 128), bf16),
+            pltpu.VMEM((2, NX, NX, CHUNKS * HALF, 8, 128), bf16),
             pltpu.VMEM((2, NX, NX, 128, 128), bf16),
             pltpu.VMEM((EXPERTS, PAD, 256), bf16),
             pltpu.VMEM((EXPERTS, PAD, 256), bf16),
-            pltpu.VMEM((MOST, 256), f32),
-            pltpu.VMEM((MOST, 128), f32),
             pltpu.VMEM((D, 256), bf16),
             pltpu.VMEM((QDIM, 256), bf16),
             pltpu.VMEM((QDIM, 256), bf16),
-            sem((7,)),
+            sem((10,)),
             sem((CHUNKS,)),
             sem((1,)),
             sem((2 * CHUNKS + 1, 6)),

time: 93 us -> 89.7 us (0.965)
  Pallas kernels: 90.9 us -> 87.6 us
    pallas_call x1, Pallas kernels: 90.9 us -> 87.6 us  [shards(): pl.pallas_call(kernel, out_shape=(pltpu.VMEM((TOK, 256), bf16), pltpu.VME...]
where the time goes in v2:
time: 89.7 us; the launch traced here: 89.5 us
  Pallas kernels  87.6 us (98%)
  local copies, waits for them, and re-layouts  1.31 us (1%)
    pallas_call x1, Pallas kernels, shards(): pl.pallas_call(kernel, out_shape=(pltpu.VMEM((TOK, 256), bf16), pltpu.VME...  87.6 us

profile of v2, /device:TPU:1, one launch (start us, length us, event | category | flops | bytes accessed | tf_op | source)
XLA Modules:
  0.0 89.5 jit_solution(14614952857511961240)
XLA Ops:
  0.6 87.6 %shard_map.167 = (bf16[256,256]{1,0:T(8,128)(2,1)S(1)}, bf16[256,256]{1,0:T(8,128)(2,1)S(1)}) custom-call(s32[2,256]{1,0:T(2,128)} %bitcast.12, bf16[256,256]{1,0:T(8,128)(2,1)} %refs_1_.1, bf16[256,128]{1,0:T(8,128)(2,1)} %refs_2_.1, bf16[64,256]{1,0:T(8,128)(2,1)} %bitcast.8, bf16[64,256]{1,0:T(8,128)(2,1)} %bitcast.9, f32[1,64]{1,0:T(1,128)} %bitcast.14, ...), custom_call_target="tpu_custom_call" | custom-call | tf_op jit(solution)/shard_map/pallas_call | solution.py:450
  88.2 0.7 copy.20
  88.9 0.7 copy.21
